TPU v7x, 32 devices: a whole 2x2x4 slice. The times are simulated.
32 devices in a mesh: ep: 16 (over z, y, x), tp: 2 (over core).
Axes of the slice: x: 2, y: 2, z: 4, core: 2. Of those that a mesh axis runs over, the one named last changes fastest.
Arguments:
- tokens: bfloat16 [384, 4096], P('ep'), may hold values from -6 to 6
- in_gain: float32 [4096], replicated, may hold values from 0.1 to 1.9
- routes: int32 [384, 6], P('ep'), may hold values from 0 to 15, all different within a row; in each aligned block of 24 rows (0 to 23, 24 to 47, ...) at most 10 rows name the same one
- gates: float32 [384, 6], P('ep'), may hold values from 0.25 to 1.5
- expert_gate: bfloat16 [16, 512, 4096], P('ep', 'tp'), may hold values from -0.09375 to 0.09375
- expert_up: bfloat16 [16, 512, 4096], P('ep', 'tp'), may hold values from -0.09375 to 0.09375
- expert_down: bfloat16 [16, 512, 4096], P('ep', None, 'tp'), may hold values from -0.25 to 0.25
- shared_gate: bfloat16 [512, 4096], P('tp'), may hold values from -0.09375 to 0.09375
- shared_up: bfloat16 [512, 4096], P('tp'), may hold values from -0.09375 to 0.09375
- shared_down: bfloat16 [512, 4096], P(None, 'tp')
- out_gain: float32 [4096], P('tp'), may hold values from 0.1 to 1.9
Outputs:
- mixed: bfloat16 [384, 4096], P('ep', 'tp')
Inputs may be any that keep to these rules, and one draw needn't show every extreme that they name: `routes`: each row names 6 different experts; among the 24 rows of one index of ep no expert is named more than 10 times, and on some index of ep some expert is named exactly 10 times.
All inputs are finite; a program needn't handle non-finite values.
Results may differ from a plain program's by a relative error of at most 0.0075.
Values may be sent and summed in bfloat16 or wider, within the bound.
A program may use at most 64 MiB of HBM per device.

v0:
```python
import functools

import jax
import jax.numpy as jnp
from jax import lax
from jax.experimental import pallas as pl
from jax.experimental.pallas import tpu as pltpu
from jax.sharding import PartitionSpec as P

EPS = 1e-06
MESH = pl.DeviceIdType.MESH
F32 = jnp.float32
BF16 = jnp.bfloat16


def dot_nt(a, b):
    return lax.dot_general(a, b, (((1,), (1,)), ((), ())), preferred_element_type=F32)


def dot_nn(a, b):
    return jnp.dot(a, b, preferred_element_type=F32)


def silu_mul(g, u):
    return g / (1.0 + jnp.exp(-g)) * u


def kernel(
    experts, fulls, rest,
    tok, ing, routes, gates, eg, eu, ed, sg, su, sd, outg,
    o,
    vg, vu, vd, vsg, vsu, vsd,
    nrm, send, recv, acc_g, acc_u, sacc_g, sacc_u, hbuf, shbuf, outb, ret, comb, sq,
    wsem, lsem, dsend, drecv, fsend, frecv, rsend, rrecv, xsend, xrecv,
):
    me = lax.axis_index("ep")
    tp = lax.axis_index("tp")
    rows, width = tok.shape
    group = lax.axis_size("tp")
    half = width // group
    slots = experts * 8
    folds = 8 // rest if rest else 1
    kc = half // folds if rest else min(512, half)
    blocks = fulls + (1 if rest else 0)

    loads = [
        pltpu.make_async_copy(src, dst, wsem.at[i])
        for i, (src, dst) in enumerate(
            ((sg, vsg), (su, vsu), (eg.at[0], vg), (eu.at[0], vu), (ed.at[0], vd), (sd, vsd))
        )
    ]
    for load in loads:
        load.start()

    barrier = pltpu.get_barrier_semaphore()

    @pl.loop(1, experts)
    def _(k):
        pl.semaphore_signal(
            barrier, inc=1, device_id=(lax.rem(me + k, experts), tp), device_id_type=MESH
        )

    for q in range(1, group):
        pl.semaphore_signal(
            barrier, inc=1, device_id=(me, lax.rem(tp + q, group)), device_id_type=MESH
        )

    x = tok[...].astype(F32)
    scale = lax.rsqrt(jnp.mean(x * x, axis=1, keepdims=True) + EPS)

    def normalize(part):
        cols = pl.ds(pl.multiple_of(part * half, half), half)
        nrm[part] = (tok[:, cols].astype(F32) * scale * ing[:, cols]).astype(BF16)

    normalize(tp)

    expert_ids = lax.broadcasted_iota(jnp.int32, (experts, rows), 0)
    chosen_t = jnp.zeros((experts, rows), F32)
    weight_t = jnp.zeros((experts, rows), F32)
    for k in range(routes.shape[0]):
        hit = routes[k : k + 1, :] == expert_ids
        chosen_t = jnp.where(hit, 1.0, chosen_t)
        weight_t = jnp.where(hit, gates[k : k + 1, :], weight_t)
    chosen_t = chosen_t.astype(BF16)
    token_r = lax.broadcasted_iota(jnp.int32, (rows, rows), 0)
    token_c = lax.broadcasted_iota(jnp.int32, (rows, rows), 1)
    earlier = (token_r < token_c).astype(F32).astype(BF16)
    rank_t = dot_nn(chosen_t, earlier).astype(BF16)

    def places(slot):
        row = slot % 8
        listed = [((8 * i + row).astype(F32), None) for i in range(fulls)]
        if rest:
            listed.append(((8 * fulls + row % rest).astype(F32), row // rest))
        return listed

    spread_t = (
        lax.broadcasted_iota(jnp.int32, (slots, experts), 0) // 8
        == lax.broadcasted_iota(jnp.int32, (slots, experts), 1)
    ).astype(F32).astype(BF16)
    named_t = dot_nn(spread_t, chosen_t) > 0.5
    ranks_t = dot_nn(spread_t, rank_t)
    for i, (place, piece) in enumerate(
        places(lax.broadcasted_iota(jnp.int32, (slots, rows), 0))
    ):
        here = jnp.where(named_t & (ranks_t == place), 1.0, 0.0)
        if piece is None:
            here = here.astype(BF16)
            for c in range(half // kc):
                send[:, i * half + c * kc : i * half + (c + 1) * kc] = dot_nn(
                    here, nrm[tp, :, c * kc : (c + 1) * kc]
                ).astype(BF16)
        else:
            send[:, i * half : i * half + kc] = sum(
                dot_nn(
                    jnp.where(piece == c, here, 0.0).astype(BF16),
                    nrm[tp, :, c * kc : (c + 1) * kc],
                )
                for c in range(folds)
            ).astype(BF16)

    def own_rows(expert):
        return pl.ds(pl.multiple_of(expert * 8, 8), 8)

    pl.semaphore_wait(barrier, experts - 1 + group - 1)

    def dispatch(dest, source):
        return pltpu.make_async_remote_copy(
            src_ref=send.at[own_rows(dest)],
            dst_ref=recv.at[tp, own_rows(source)],
            send_sem=dsend.at[dest],
            recv_sem=drecv.at[source],
            device_id=(dest, tp),
            device_id_type=MESH,
        )

    def forward(part, source, q):
        return pltpu.make_async_remote_copy(
            src_ref=recv.at[part, own_rows(source)],
            dst_ref=recv.at[part, own_rows(source)],
            send_sem=fsend.at[q, source],
            recv_sem=frecv.at[part, source],
            device_id=(me, lax.rem(tp + q, group)),
            device_id_type=MESH,
        )

    def give_back(dest, source):
        return pltpu.make_async_remote_copy(
            src_ref=outb.at[own_rows(dest)],
            dst_ref=ret.at[own_rows(source)],
            send_sem=rsend.at[dest],
            recv_sem=rrecv.at[source],
            device_id=(dest, tp),
            device_id_type=MESH,
        )

    def swap(ref, i, part, q):
        return pltpu.make_async_remote_copy(
            src_ref=ref.at[part],
            dst_ref=ref.at[part],
            send_sem=xsend.at[i, q],
            recv_sem=xrecv.at[i, part],
            device_id=(me, lax.rem(tp + q, group)),
            device_id_type=MESH,
        )

    def swap_start(ref, i):
        for q in range(1, group):
            swap(ref, i, tp, q).start()

    def swap_recv(ref, i):
        for q in range(1, group):
            swap(ref, i, lax.rem(tp + q, group), q).wait_recv()

    def swap_sent(ref, i):
        for q in range(1, group):
            swap(ref, i, tp, q).wait_send()

    def forward_start(source):
        for q in range(1, group):
            forward(tp, source, q).start()

    @pl.loop(1, experts)
    def _(k):
        dispatch(lax.rem(me + k, experts), me).start()

    own = pltpu.make_async_copy(
        send.at[own_rows(me)], recv.at[tp, own_rows(me)], lsem.at[0]
    )
    own.start()

    for q in range(1, group):
        normalize(lax.rem(tp + q, group))
    loads[0].wait()
    loads[1].wait()
    sacc_g[...] = jnp.zeros_like(sacc_g)
    sacc_u[...] = jnp.zeros_like(sacc_u)
    for h in range(group):

        @pl.loop(0, half // kc)
        def _(c):
            cols = pl.ds(pl.multiple_of(c * kc, kc), kc)
            wide = pl.ds(pl.multiple_of(h * half + c * kc, kc), kc)
            xs = nrm[h, :, cols]
            sacc_g[...] += dot_nt(xs, vsg[:, wide])
            sacc_u[...] += dot_nt(xs, vsu[:, wide])

    shbuf[tp] = silu_mul(sacc_g[...], sacc_u[...]).astype(BF16)
    swap_start(shbuf, 0)

    own.wait()
    forward_start(me)

    @pl.loop(1, experts)
    def _(k):
        source = lax.rem(me + experts - k, experts)
        dispatch(source, source).wait_recv()
        forward_start(source)

    loads[2].wait()
    loads[3].wait()
    acc_g[...] = jnp.zeros_like(acc_g)
    acc_u[...] = jnp.zeros_like(acc_u)

    if rest:
        row_piece = lax.broadcasted_iota(jnp.int32, (slots, kc), 0) % 8 // rest

    def project_part(part):
        @pl.loop(0, half // kc)
        def _(c):
            cols = pl.ds(pl.multiple_of(c * kc, kc), kc)
            wide = pl.ds(pl.multiple_of(part * half + c * kc, kc), kc)
            pieces = [
                recv[part, :, pl.ds(pl.multiple_of(i * half + c * kc, kc), kc)]
                for i in range(fulls)
            ]
            if rest:
                last = recv[part, :, fulls * half : fulls * half + kc]
                pieces.append(jnp.where(row_piece == c, last, jnp.zeros_like(last)))
            xs = jnp.concatenate(pieces, axis=0)
            acc_g[...] += dot_nt(xs, vg[:, wide])
            acc_u[...] += dot_nt(xs, vu[:, wide])

    project_part(tp)

    for q in range(1, group):
        part = lax.rem(tp + q, group)

        @pl.loop(0, experts)
        def _(k):
            forward(part, lax.rem(me + experts - k, experts), q).wait_recv()

        project_part(part)

    for i in range(blocks):
        block = slice(i * slots, (i + 1) * slots)
        g, u = acc_g[block], acc_u[block]
        if i == fulls:
            g = g.reshape(experts, 8, -1)
            u = u.reshape(experts, 8, -1)
            shift = rest
            while shift < 8:
                g = g + pltpu.roll(g, shift, 1)
                u = u + pltpu.roll(u, shift, 1)
                shift *= 2
            g = g.reshape(slots, -1)
            u = u.reshape(slots, -1)
        hbuf[tp, block] = silu_mul(g, u).astype(BF16)
    swap_start(hbuf, 1)
    loads[4].wait()
    swap_recv(hbuf, 1)

    def down(hidden, weights, cols):
        depth = weights.shape[0] // group
        return sum(
            dot_nn(hidden[p], weights[p * depth : (p + 1) * depth, cols]) for p in range(group)
        )

    for c in range(half // kc):
        cols = slice(c * kc, (c + 1) * kc)
        made = down(hbuf, vd, cols)
        for i in range(fulls):
            outb[:, i * half + c * kc : i * half + (c + 1) * kc] = made[
                i * slots : (i + 1) * slots
            ].astype(BF16)
        if rest:
            fresh = made[fulls * slots :]
            last = fresh if c == 0 else jnp.where(row_piece == c, fresh, last)
    if rest:
        outb[:, fulls * half :] = last.astype(BF16)

    @pl.loop(1, experts)
    def _(k):
        give_back(lax.rem(me + k, experts), me).start()

    own_back = pltpu.make_async_copy(
        outb.at[own_rows(me)], ret.at[own_rows(me)], lsem.at[1]
    )
    own_back.start()

    loads[5].wait()
    swap_recv(shbuf, 0)
    for c in range(half // kc):
        cols = slice(c * kc, (c + 1) * kc)
        comb[:, cols] = down(shbuf, vsd, cols)
    spread = (
        lax.broadcasted_iota(jnp.int32, (experts, slots), 1) // 8
        == lax.broadcasted_iota(jnp.int32, (experts, slots), 0)
    ).astype(F32).astype(BF16)
    eye = (token_r == token_c).astype(F32).astype(BF16)
    coarse_t = weight_t.astype(BF16)
    fine_t = (weight_t - coarse_t.astype(F32)).astype(BF16)
    named, ranks, coarse, fine = [
        dot_nn(dot_nt(eye, t).astype(BF16), spread) for t in (chosen_t, rank_t, coarse_t, fine_t)
    ]
    mixing = []
    for place, piece in places(lax.broadcasted_iota(jnp.int32, (rows, slots), 1)):
        taken = (named > 0.5) & (ranks == place)
        mixing.append((taken, piece))

    own_back.wait()

    @pl.loop(1, experts)
    def _(k):
        source = lax.rem(me + experts - k, experts)
        give_back(source, source).wait_recv()

    total = jnp.zeros((rows, 1), F32)
    for c in range(half // kc):
        cols = slice(c * kc, (c + 1) * kc)
        part = comb[:, cols]
        for i, (taken, piece) in enumerate(mixing):
            if piece is None:
                back = ret[:, i * half + c * kc : i * half + (c + 1) * kc]
            else:
                back = ret[:, i * half : i * half + kc]
                taken = taken & (piece == c)
            both = jnp.concatenate(
                [jnp.where(taken, coarse, 0.0), jnp.where(taken, fine, 0.0)], axis=0
            )
            mixed = dot_nn(both.astype(BF16), back)
            part += mixed[:rows] + mixed[rows:]
        comb[:, cols] = part
        total = total + jnp.sum(part * part, axis=1, keepdims=True)
    sq[tp] = jnp.broadcast_to(total, sq.shape[1:])
    swap_start(sq, 2)

    @pl.loop(1, experts)
    def _(k):
        dest = lax.rem(me + k, experts)
        dispatch(dest, me).wait_send()
        give_back(dest, me).wait_send()

    @pl.loop(0, experts)
    def _(k):
        for q in range(1, group):
            forward(tp, k, q).wait_send()

    swap_sent(shbuf, 0)
    swap_sent(hbuf, 1)
    swap_recv(sq, 2)
    norm = lax.rsqrt(sum(sq[p] for p in range(group))[:, :1] / width + EPS)
    o[...] = (comb[...] * norm * outg[...]).astype(BF16)
    swap_sent(sq, 2)


def on_device(experts, tokens, in_gain, routes, gates, eg, eu, ed, sg, su, sd, out_gain):
    rows, width = tokens.shape
    group = lax.axis_size("tp")
    half = width // group
    cap = min(rows, (rows * routes.shape[1] + experts - 1) // experts + 1)
    fulls, rest = cap // 8, cap % 8
    while rest & (rest - 1):
        rest += 1
    if rest and half * rest // 8 % 128:
        rest = 8
    if rest == 8:
        fulls, rest = fulls + 1, 0
    slots = experts * 8
    blocks = fulls + (1 if rest else 0)
    packed = fulls * half + half * rest // 8
    hid, shid = eg.shape[1], sg.shape[0]
    vmem = pl.BlockSpec(memory_space=pltpu.VMEM)
    hbm = pl.BlockSpec(memory_space=pl.ANY)
    dma = pltpu.SemaphoreType.DMA
    return pl.pallas_call(
        functools.partial(kernel, experts, fulls, rest),
        out_shape=jax.ShapeDtypeStruct((rows, half), BF16),
        in_specs=[vmem] * 4 + [hbm] * 6 + [vmem],
        out_specs=vmem,
        scratch_shapes=[
            pltpu.VMEM(eg.shape[1:], BF16),
            pltpu.VMEM(eu.shape[1:], BF16),
            pltpu.VMEM(ed.shape[1:], BF16),
            pltpu.VMEM(sg.shape, BF16),
            pltpu.VMEM(su.shape, BF16),
            pltpu.VMEM(sd.shape, BF16),
            pltpu.VMEM((group, rows, half), BF16),
            pltpu.VMEM((slots, packed), BF16),
            pltpu.VMEM((group, slots, packed), BF16),
            pltpu.VMEM((blocks * slots, hid), F32),
            pltpu.VMEM((blocks * slots, hid), F32),
            pltpu.VMEM((rows, shid), F32),
            pltpu.VMEM((rows, shid), F32),
            pltpu.VMEM((group, blocks * slots, hid), BF16),
            pltpu.VMEM((group, rows, shid), BF16),
            pltpu.VMEM((slots, packed), BF16),
            pltpu.VMEM((slots, packed), BF16),
            pltpu.VMEM((rows, half), F32),
            pltpu.VMEM((group, rows, 128), F32),
            dma((6,)),
            dma((2,)),
            dma((experts,)),
            dma((experts,)),
            dma((group, experts)),
            dma((group, experts)),
            dma((experts,)),
            dma((experts,)),
            dma((3, group)),
            dma((3, group)),
        ],
        compiler_params=pltpu.CompilerParams(
            collective_id=0, has_side_effects=True, vmem_limit_bytes=60 * 1024 * 1024
        ),
    )(
        tokens, in_gain.reshape(1, width), routes.T, gates.T, eg, eu, ed, sg, su, sd,
        out_gain.reshape(1, half),
    )


def solution(mesh):
    in_specs = (
        P("ep", None),
        P(),
        P("ep", None),
        P("ep", None),
        P("ep", "tp", None),
        P("ep", "tp", None),
        P("ep", None, "tp"),
        P("tp", None),
        P("tp", None),
        P(None, "tp"),
        P("tp"),
    )
    return jax.shard_map(
        functools.partial(on_device, mesh.shape["ep"]),
        mesh=mesh,
        in_specs=in_specs,
        out_specs=P("ep", "tp"),
        check_vma=False,
    )
```

profile of v0, /device:TPU:29, one launch (start us, length us, event | category | flops | bytes accessed | tf_op | source)
XLA Modules:
  0.0 46.2 jit_solution(8303957775887837785)
XLA Ops:
  0.0 44.7 %shard_map.109 = bf16[24,2048]{1,0:T(8,128)(2,1)} custom-call(bf16[24,4096]{1,0:T(8,128)(2,1)} %tok.1, f32[1,4096]{1,0:T(1,128)} %bitcast.4, s32[6,24]{1,0:T(8,128)} %bitcast.6, f32[6,24]{1,0:T(8,128)} %bitcast.7, bf16[1,256,4096]{2,1,0:T(8,128)(2,1)} %eg.1, bf16[1,256,4096]{2,1,0:T(8,128)(2,1)} %eu.1, bf16[1,512,2048]{2,1,0:T(8,128)(2,1)} %ed.1, ...), custom_call_target="tpu_custom_call" | custom-call | tf_op jit(solution)/shard_map/pallas_call | solution.py:386
  44.7 1.5 %copy.13 = bf16[24,2048]{1,0:T(8,128)(2,1)} copy(bf16[24,2048]{1,0:T(8,128)(2,1)} %shard_map.109) | data formatting | bytes 196608
where the time goes:
time: 46.4 us; the launch traced here: 46.2 us
  Pallas kernels  44.7 us (96%)
  local copies, waits for them, and re-layouts  1.54 us (3%)
    pallas_call x1, Pallas kernels, on_device(): pl.pallas_call(functools.partial(kernel, experts, fulls, rest), out_shape...  44.7 us
    unnamed x1, local copies, waits for them, and re-layouts  1.54 us

commit v1 on v0

v1 whole, which is shorter than its diff:
```python
import functools

import jax
import jax.numpy as jnp
from jax import lax
from jax.experimental import pallas as pl
from jax.experimental.pallas import tpu as pltpu
from jax.sharding import PartitionSpec as P

EPS = 1e-06
MESH = pl.DeviceIdType.MESH
F32 = jnp.float32
BF16 = jnp.bfloat16
OWN, FAR = 0, 1
SHARED, HIDDEN, SQUARES = 0, 1, 3


def dot_nt(a, b):
    return lax.dot_general(a, b, (((1,), (1,)), ((), ())), preferred_element_type=F32)


def dot_nn(a, b):
    return jnp.dot(a, b, preferred_element_type=F32)


def silu_mul(g, u):
    return g / (1.0 + jnp.exp(-g)) * u


def kernel(
    experts, fulls, rest, chunks,
    tok_h, ing_h, routes_h, gates_h, eg, eu, ed, sg, su, sd, outg_h,
    o,
    tok, ing, routes, gates, outg,
    vg, vu, vd, vsg, vsu, vsd,
    nrm, far_x, info, far_info, send, recv, acc_g, acc_u, hbuf, shbuf, outb, ret, psend, precv, comb, sq,
    isem, wsem, lsem, csend, crecv, dsend, drecv, fsend, frecv, rsend, rrecv, psent, pgot, xsend, xrecv,
):
    me = lax.axis_index("ep")
    tp = lax.axis_index("tp")
    rows, width = tok.shape
    group = lax.axis_size("tp")
    half = width // group
    mates = experts // 2
    side = me // mates
    spot = lax.rem(me, mates)
    pal = lax.rem(me + mates, experts)
    slots = mates * 8
    span = half // chunks
    folds = 8 // rest if rest else 1
    kc = span // folds if rest else min(512, span)
    blocks = fulls + (1 if rest else 0)

    def mate(k):
        return side * mates + k

    def turn(k):
        return lax.rem(spot + k, mates)

    barrier = pltpu.get_barrier_semaphore()

    @pl.loop(1, mates)
    def _(k):
        pl.semaphore_signal(
            barrier, inc=1, device_id=(mate(turn(k)), tp), device_id_type=MESH
        )

    pl.semaphore_signal(barrier, inc=1, device_id=(pal, tp), device_id_type=MESH)
    for q in range(1, group):
        pl.semaphore_signal(
            barrier, inc=1, device_id=(me, lax.rem(tp + q, group)), device_id_type=MESH
        )

    smalls = [
        pltpu.make_async_copy(src, dst, isem.at[i])
        for i, (src, dst) in enumerate(
            ((tok_h, tok), (ing_h, ing), (routes_h, routes), (gates_h, gates), (outg_h, outg))
        )
    ]
    loads = [
        pltpu.make_async_copy(src, dst, wsem.at[i])
        for i, (src, dst) in enumerate(
            ((sg, vsg), (su, vsu), (eg.at[0], vg), (eu.at[0], vu), (ed.at[0], vd), (sd, vsd))
        )
    ]
    for load in smalls + loads:
        load.start()

    smalls[2].wait()
    smalls[3].wait()
    expert_ids = lax.broadcasted_iota(jnp.int32, (mates, rows), 0)

    def weights_for(first):
        weight_t = jnp.zeros((mates, rows), F32)
        for k in range(routes.shape[0]):
            hit = routes[k : k + 1, :] == expert_ids + first
            weight_t = jnp.where(hit, gates[k : k + 1, :], weight_t)
        return weight_t

    own_weight = weights_for(side * mates)
    info[...] = jnp.zeros_like(info)
    info[:, :rows] = weights_for((1 - side) * mates)

    smalls[0].wait()
    smalls[1].wait()
    x = tok[...].astype(F32)
    scale = lax.rsqrt(jnp.mean(x * x, axis=1, keepdims=True) + EPS)

    def normalize(part):
        cols = pl.ds(pl.multiple_of(part * half, half), half)
        nrm[part] = (tok[:, cols].astype(F32) * scale * ing[:, cols]).astype(BF16)

    normalize(tp)

    token_r = lax.broadcasted_iota(jnp.int32, (rows, rows), 0)
    token_c = lax.broadcasted_iota(jnp.int32, (rows, rows), 1)
    earlier = (token_r < token_c).astype(F32).astype(BF16)
    eye = (token_r == token_c).astype(F32).astype(BF16)
    spread_t = (
        lax.broadcasted_iota(jnp.int32, (slots, mates), 0) // 8
        == lax.broadcasted_iota(jnp.int32, (slots, mates), 1)
    ).astype(F32).astype(BF16)
    spread = (
        lax.broadcasted_iota(jnp.int32, (mates, slots), 1) // 8
        == lax.broadcasted_iota(jnp.int32, (mates, slots), 0)
    ).astype(F32).astype(BF16)

    def places(slot):
        row = slot % 8
        listed = [((8 * i + row).astype(F32), None) for i in range(fulls)]
        if rest:
            listed.append(((8 * fulls + row % rest).astype(F32), row // rest))
        return listed

    def ranked(weight_t):
        chosen_t = jnp.where(weight_t > 0.0, 1.0, 0.0).astype(BF16)
        return chosen_t, dot_nn(chosen_t, earlier).astype(BF16)

    def pickers(weight_t):
        chosen_t, rank_t = ranked(weight_t)
        named = dot_nn(spread_t, chosen_t) > 0.5
        ranks = dot_nn(spread_t, rank_t)
        made = []
        for place, piece in places(lax.broadcasted_iota(jnp.int32, (slots, rows), 0)):
            here = jnp.where(named & (ranks == place), 1.0, 0.0)
            if piece is None:
                made.append(here.astype(BF16))
            else:
                made.append([jnp.where(piece == c, here, 0.0).astype(BF16) for c in range(folds)])
        return made

    def mixers(weight_t):
        chosen_t, rank_t = ranked(weight_t)
        coarse_t = weight_t.astype(BF16)
        fine_t = (weight_t - coarse_t.astype(F32)).astype(BF16)
        named, ranks, coarse, fine = [
            dot_nn(dot_nt(eye, t).astype(BF16), spread)
            for t in (chosen_t, rank_t, coarse_t, fine_t)
        ]
        made = []
        for place, piece in places(lax.broadcasted_iota(jnp.int32, (rows, slots), 1)):
            made.append(((named > 0.5) & (ranks == place), piece))
        return made, coarse, fine

    def pick(picker, source, s, ch):
        for i in range(fulls):
            for c in range(span // kc):
                send[s, ch, :, i * span + c * kc : i * span + (c + 1) * kc] = dot_nn(
                    picker[i], source(ch * span + c * kc)
                ).astype(BF16)
        if rest:
            send[s, ch, :, fulls * span :] = sum(
                dot_nn(picker[fulls][c], source(ch * span + c * kc)) for c in range(folds)
            ).astype(BF16)

    own_picker = pickers(own_weight)
    for ch in range(chunks):
        pick(own_picker, lambda at: nrm[tp, :, at : at + kc], OWN, ch)

    def block(index):
        return pl.ds(pl.multiple_of(index * 8, 8), 8)

    def cross_info():
        return pltpu.make_async_remote_copy(
            src_ref=info, dst_ref=far_info, send_sem=csend.at[chunks], recv_sem=crecv.at[chunks],
            device_id=(pal, tp), device_id_type=MESH,
        )

    def cross(ch):
        cols = pl.ds(ch * span, span)
        return pltpu.make_async_remote_copy(
            src_ref=nrm.at[tp, :, cols], dst_ref=far_x.at[:, cols],
            send_sem=csend.at[ch], recv_sem=crecv.at[ch],
            device_id=(pal, tp), device_id_type=MESH,
        )

    def cross_back(ch):
        cols = pl.ds(ch * span, span)
        return pltpu.make_async_remote_copy(
            src_ref=psend.at[:, cols], dst_ref=precv.at[:, cols],
            send_sem=psent.at[ch], recv_sem=pgot.at[ch],
            device_id=(pal, tp), device_id_type=MESH,
        )

    def dispatch(s, ch, dest, source):
        return pltpu.make_async_remote_copy(
            src_ref=send.at[s, ch, block(dest)],
            dst_ref=recv.at[tp, s, ch, block(source)],
            send_sem=dsend.at[s, ch, dest],
            recv_sem=drecv.at[s, ch, source],
            device_id=(mate(dest), tp),
            device_id_type=MESH,
        )

    def stay(s, ch):
        return pltpu.make_async_copy(
            send.at[s, ch, block(spot)], recv.at[tp, s, ch, block(spot)], lsem.at[0, s, ch]
        )

    def forward(part, s, ch, source, q):
        return pltpu.make_async_remote_copy(
            src_ref=recv.at[part, s, ch, block(source)],
            dst_ref=recv.at[part, s, ch, block(source)],
            send_sem=fsend.at[q, s, ch, source],
            recv_sem=frecv.at[part, s, ch, source],
            device_id=(me, lax.rem(tp + q, group)),
            device_id_type=MESH,
        )

    def give_back(s, ch, dest, source):
        return pltpu.make_async_remote_copy(
            src_ref=outb.at[s, ch, block(dest)],
            dst_ref=ret.at[s, ch, block(source)],
            send_sem=rsend.at[s, ch, dest],
            recv_sem=rrecv.at[s, ch, source],
            device_id=(mate(dest), tp),
            device_id_type=MESH,
        )

    def stay_back(s, ch):
        return pltpu.make_async_copy(
            outb.at[s, ch, block(spot)], ret.at[s, ch, block(spot)], lsem.at[1, s, ch]
        )

    def swap(view, i, part, q):
        return pltpu.make_async_remote_copy(
            src_ref=view(part),
            dst_ref=view(part),
            send_sem=xsend.at[i, q],
            recv_sem=xrecv.at[i, part],
            device_id=(me, lax.rem(tp + q, group)),
            device_id_type=MESH,
        )

    def swap_start(view, i):
        for q in range(1, group):
            swap(view, i, tp, q).start()

    def swap_recv(view, i):
        for q in range(1, group):
            swap(view, i, lax.rem(tp + q, group), q).wait_recv()

    def swap_sent(view, i):
        for q in range(1, group):
            swap(view, i, tp, q).wait_send()

    def hidden_view(s):
        return lambda part: hbuf.at[part, s]

    def shared_view(part):
        return shbuf.at[part]

    def squares_view(part):
        return sq.at[part]

    def scatter(s, ch):
        @pl.loop(1, mates)
        def _(k):
            dispatch(s, ch, turn(k), spot).start()

        stay(s, ch).start()

    def pass_on(s, ch):
        stay(s, ch).wait()
        for q in range(1, group):
            forward(tp, s, ch, spot, q).start()

        @pl.loop(1, mates)
        def _(k):
            source = turn(mates - k)
            dispatch(s, ch, source, source).wait_recv()
            for q in range(1, group):
                forward(tp, s, ch, source, q).start()

    def passed(s, part, q):
        for ch in range(chunks):

            @pl.loop(0, mates)
            def _(k):
                forward(part, s, ch, turn(mates - k), q).wait_recv()

    pl.semaphore_wait(barrier, mates - 1 + 1 + group - 1)

    cross_info().start()
    for ch in range(chunks):
        cross(ch).start()
    for ch in range(chunks):
        scatter(OWN, ch)

    for q in range(1, group):
        normalize(lax.rem(tp + q, group))
    loads[0].wait()
    loads[1].wait()
    wide_k = min(512, half)
    acc_g[0, :rows] = jnp.zeros((rows, vsg.shape[0]), F32)
    acc_u[0, :rows] = jnp.zeros((rows, vsu.shape[0]), F32)
    for h in range(group):

        @pl.loop(0, half // wide_k)
        def _(c):
            cols = pl.ds(pl.multiple_of(c * wide_k, wide_k), wide_k)
            wide = pl.ds(pl.multiple_of(h * half + c * wide_k, wide_k), wide_k)
            xs = nrm[h, :, cols]
            acc_g[0, :rows] += dot_nt(xs, vsg[:, wide])
            acc_u[0, :rows] += dot_nt(xs, vsu[:, wide])

    shbuf[tp] = silu_mul(acc_g[0, :rows], acc_u[0, :rows]).astype(BF16)
    swap_start(shared_view, SHARED)

    cross_info().wait_recv()
    far_weight = far_info[:, :rows]
    far_picker = pickers(far_weight)
    for ch in range(chunks):
        cross(ch).wait_recv()
        pick(far_picker, lambda at: far_x[:, at : at + kc], FAR, ch)
        scatter(FAR, ch)

    row_piece = lax.broadcasted_iota(jnp.int32, (slots, kc), 0) % 8 // rest if rest else None

    def project(s, part, first):
        for ch in range(chunks):
            pieces = [recv[part, s, ch, :, i * span : (i + 1) * span] for i in range(fulls)]
            if rest:
                last = recv[part, s, ch, :, fulls * span :]
                pieces.append(
                    jnp.concatenate(
                        [jnp.where(row_piece == c, last, jnp.zeros_like(last)) for c in range(folds)],
                        axis=1,
                    )
                )
            xs = jnp.concatenate(pieces, axis=0)
            wide = pl.ds(pl.multiple_of(part * half + ch * span, span), span)
            g = dot_nt(xs, vg[:, wide])
            u = dot_nt(xs, vu[:, wide])
            if first and ch == 0:
                acc_g[s] = g
                acc_u[s] = u
            else:
                acc_g[s] += g
                acc_u[s] += u

    def activate(s):
        for i in range(blocks):
            at = slice(i * slots, (i + 1) * slots)
            g, u = acc_g[s, at], acc_u[s, at]
            if i == fulls:
                g = g.reshape(mates, 8, -1)
                u = u.reshape(mates, 8, -1)
                shift = rest
                while shift < 8:
                    g = g + pltpu.roll(g, shift, 1)
                    u = u + pltpu.roll(u, shift, 1)
                    shift *= 2
                g = g.reshape(slots, -1)
                u = u.reshape(slots, -1)
            hbuf[tp, s, at] = silu_mul(g, u).astype(BF16)
        swap_start(hidden_view(s), HIDDEN + s)

    def down(hidden, weights, at):
        depth = weights.shape[0] // group
        return sum(
            dot_nn(hidden(p), weights[p * depth : (p + 1) * depth, at : at + kc])
            for p in range(group)
        )

    def respond(s):
        for ch in range(chunks):
            for c in range(span // kc):
                made = down(lambda p: hbuf[p, s], vd, ch * span + c * kc)
                for i in range(fulls):
                    outb[s, ch, :, i * span + c * kc : i * span + (c + 1) * kc] = made[
                        i * slots : (i + 1) * slots
                    ].astype(BF16)
                if rest:
                    fresh = made[fulls * slots :]
                    last = fresh if c == 0 else jnp.where(row_piece == c, fresh, last)
            if rest:
                outb[s, ch, :, fulls * span :] = last.astype(BF16)

            @pl.loop(1, mates)
            def _(k):
                give_back(s, ch, turn(k), spot).start()

            stay_back(s, ch).start()

    for ch in range(chunks):
        pass_on(OWN, ch)
    loads[2].wait()
    loads[3].wait()
    project(OWN, tp, True)
    for q in range(1, group):
        part = lax.rem(tp + q, group)
        passed(OWN, part, q)
        project(OWN, part, False)
    activate(OWN)

    for ch in range(chunks):
        pass_on(FAR, ch)
    project(FAR, tp, True)
    loads[4].wait()
    swap_recv(hidden_view(OWN), HIDDEN + OWN)
    respond(OWN)
    for q in range(1, group):
        part = lax.rem(tp + q, group)
        passed(FAR, part, q)
        project(FAR, part, False)
    activate(FAR)
    swap_recv(hidden_view(FAR), HIDDEN + FAR)
    respond(FAR)

    loads[5].wait()
    swap_recv(shared_view, SHARED)
    for at in range(0, half, kc):
        comb[:, at : at + kc] = down(lambda p: shbuf[p], vsd, at)

    def came_back(s, ch):
        stay_back(s, ch).wait()

        @pl.loop(1, mates)
        def _(k):
            source = turn(mates - k)
            give_back(s, ch, source, source).wait_recv()

    def mix(mixer, s, ch, c):
        listed, coarse, fine = mixer
        backs, tops, lows = [], [], []
        for i, (taken, piece) in enumerate(listed):
            if piece is None:
                backs.append(ret[s, ch, :, i * span + c * kc : i * span + (c + 1) * kc])
            else:
                backs.append(ret[s, ch, :, fulls * span :])
                taken = taken & (piece == c)
            tops.append(jnp.where(taken, coarse, 0.0))
            lows.append(jnp.where(taken, fine, 0.0))
        both = jnp.concatenate(
            [jnp.concatenate(tops, axis=1), jnp.concatenate(lows, axis=1)], axis=0
        )
        mixed = dot_nn(both.astype(BF16), jnp.concatenate(backs, axis=0))
        return mixed[:rows] + mixed[rows:]

    far_mixer = mixers(far_weight)
    for ch in range(chunks):
        came_back(FAR, ch)
        for c in range(span // kc):
            at = ch * span + c * kc
            psend[:, at : at + kc] = mix(far_mixer, FAR, ch, c).astype(BF16)
        cross_back(ch).start()

    own_mixer = mixers(own_weight)
    for ch in range(chunks):
        came_back(OWN, ch)
        for c in range(span // kc):
            at = ch * span + c * kc
            comb[:, at : at + kc] += mix(own_mixer, OWN, ch, c)

    total = jnp.zeros((rows, 1), F32)
    for ch in range(chunks):
        cross_back(ch).wait_recv()
        for c in range(span // kc):
            at = ch * span + c * kc
            part = comb[:, at : at + kc] + precv[:, at : at + kc].astype(F32)
            comb[:, at : at + kc] = part
            total = total + jnp.sum(part * part, axis=1, keepdims=True)
    sq[tp] = jnp.broadcast_to(total, sq.shape[1:])
    swap_start(squares_view, SQUARES)

    cross_info().wait_send()
    for ch in range(chunks):
        cross(ch).wait_send()
        cross_back(ch).wait_send()
        for s in (OWN, FAR):

            @pl.loop(1, mates)
            def _(k):
                dispatch(s, ch, turn(k), spot).wait_send()
                give_back(s, ch, turn(k), spot).wait_send()

            @pl.loop(0, mates)
            def _(k):
                for q in range(1, group):
                    forward(tp, s, ch, k, q).wait_send()

    swap_sent(shared_view, SHARED)
    for s in (OWN, FAR):
        swap_sent(hidden_view(s), HIDDEN + s)
    smalls[4].wait()
    swap_recv(squares_view, SQUARES)
    norm = lax.rsqrt(sum(sq[p] for p in range(group))[:, :1] / width + EPS)
    o[...] = (comb[...] * norm * outg[...]).astype(BF16)
    swap_sent(squares_view, SQUARES)


def on_device(experts, tokens, in_gain, routes, gates, eg, eu, ed, sg, su, sd, out_gain):
    rows, width = tokens.shape
    topk = routes.shape[1]
    group = lax.axis_size("tp")
    half = width // group
    cap = min(rows, (rows * topk + experts - 1) // experts + 1)
    fulls, rest = cap // 8, cap % 8
    while rest & (rest - 1):
        rest += 1
    if rest and half * rest // 8 % 128:
        rest = 8
    if rest == 8:
        fulls, rest = fulls + 1, 0
    chunks = 1 if half // 2 * (rest or 8) // 8 % 128 else 2
    mates = experts // 2
    slots = mates * 8
    blocks = fulls + (1 if rest else 0)
    span = half // chunks
    packed = fulls * span + span * rest // 8
    hid, shid = eg.shape[1], sg.shape[0]
    deep = max(blocks * slots, rows)
    vmem = pl.BlockSpec(memory_space=pltpu.VMEM)
    hbm = pl.BlockSpec(memory_space=pl.ANY)
    dma = pltpu.SemaphoreType.DMA
    sets = (2, chunks, slots, packed)
    assert deep == blocks * slots and hid == shid and mates * 2 == experts
    return pl.pallas_call(
        functools.partial(kernel, experts, fulls, rest, chunks),
        out_shape=jax.ShapeDtypeStruct((rows, half), BF16),
        in_specs=[hbm] * 11,
        out_specs=vmem,
        scratch_shapes=[
            pltpu.VMEM((rows, width), BF16),
            pltpu.VMEM((1, width), F32),
            pltpu.VMEM((topk, rows), jnp.int32),
            pltpu.VMEM((topk, rows), F32),
            pltpu.VMEM((1, half), F32),
            pltpu.VMEM(eg.shape[1:], BF16),
            pltpu.VMEM(eu.shape[1:], BF16),
            pltpu.VMEM(ed.shape[1:], BF16),
            pltpu.VMEM(sg.shape, BF16),
            pltpu.VMEM(su.shape, BF16),
            pltpu.VMEM(sd.shape, BF16),
            pltpu.VMEM((group, rows, half), BF16),
            pltpu.VMEM((rows, half), BF16),
            pltpu.VMEM((mates, 128), F32),
            pltpu.VMEM((mates, 128), F32),
            pltpu.VMEM(sets, BF16),
            pltpu.VMEM((group,) + sets, BF16),
            pltpu.VMEM((2, deep, hid), F32),
            pltpu.VMEM((2, deep, hid), F32),
            pltpu.VMEM((group, 2, blocks * slots, hid), BF16),
            pltpu.VMEM((group, rows, shid), BF16),
            pltpu.VMEM(sets, BF16),
            pltpu.VMEM(sets, BF16),
            pltpu.VMEM((rows, half), BF16),
            pltpu.VMEM((rows, half), BF16),
            pltpu.VMEM((rows, half), F32),
            pltpu.VMEM((group, rows, 128), F32),
            dma((5,)),
            dma((6,)),
            dma((2, 2, chunks)),
            dma((chunks + 1,)),
            dma((chunks + 1,)),
            dma((2, chunks, mates)),
            dma((2, chunks, mates)),
            dma((group, 2, chunks, mates)),
            dma((group, 2, chunks, mates)),
            dma((2, chunks, mates)),
            dma((2, chunks, mates)),
            dma((chunks,)),
            dma((chunks,)),
            dma((4, group)),
            dma((4, group)),
        ],
        compiler_params=pltpu.CompilerParams(
            collective_id=0, has_side_effects=True, vmem_limit_bytes=60 * 1024 * 1024
        ),
    )(
        tokens, in_gain.reshape(1, width), routes.T, gates.T, eg, eu, ed, sg, su, sd,
        out_gain.reshape(1, half),
    )


def solution(mesh):
    in_specs = (
        P("ep", None),
        P(),
        P("ep", None),
        P("ep", None),
        P("ep", "tp", None),
        P("ep", "tp", None),
        P("ep", None, "tp"),
        P("tp", None),
        P("tp", None),
        P(None, "tp"),
        P("tp"),
    )
    return jax.shard_map(
        functools.partial(on_device, mesh.shape["ep"]),
        mesh=mesh,
        in_specs=in_specs,
        out_specs=P("ep", "tp"),
        check_vma=False,
    )
```

time: 46.4 us -> 40.2 us (0.87)
  the two profiles are of different devices: /device:TPU:29 before, /device:TPU:0 now
where the time goes in v1:
time: 40.2 us; the launch traced here: 40 us
  Pallas kernels  38.5 us (96%)
  local copies, waits for them, and re-layouts  1.54 us (4%)
    pallas_call x1, Pallas kernels, on_device(): pl.pallas_call(functools.partial(kernel, experts, fulls, rest, chunks), o...  38.5 us
    unnamed x1, local copies, waits for them, and re-layouts  1.54 us

profile of v1, /device:TPU:0, one launch (start us, length us, event | category | flops | bytes accessed | tf_op | source)
XLA Modules:
  0.0 40.0 jit_solution(8364749748327941774)
XLA Ops:
  0.0 38.5 %shard_map.109 = bf16[24,2048]{1,0:T(8,128)(2,1)} custom-call(bf16[24,4096]{1,0:T(8,128)(2,1)} %tok_h.1, f32[1,4096]{1,0:T(1,128)} %bitcast.4, s32[6,24]{1,0:T(8,128)} %bitcast.6, f32[6,24]{1,0:T(8,128)} %bitcast.7, bf16[1,256,4096]{2,1,0:T(8,128)(2,1)} %eg.1, bf16[1,256,4096]{2,1,0:T(8,128)(2,1)} %eu.1, bf16[1,512,2048]{2,1,0:T(8,128)(2,1)} %ed.1, ...), custom_call_target="tpu_custom_call" | custom-call | tf_op jit(solution)/shard_map/pallas_call | solution.py:539
  38.5 1.5 %copy.13 = bf16[24,2048]{1,0:T(8,128)(2,1)} copy(bf16[24,2048]{1,0:T(8,128)(2,1)} %shard_map.109) | data formatting | bytes 196608
